TPU v7x, 32 devices: a whole 2x2x4 slice. The times are simulated.
32 devices in a mesh: sp: 8 (over z, y), tp: 4 (over x, core).
Axes of the slice: x: 2, y: 2, z: 4, core: 2. Of those that a mesh axis runs over, the one named last changes fastest.
Arguments:
- latents: bfloat16 [2560, 2048], P(('sp', 'tp')), may hold values from -12.5 to 12.5, as said below
- context: bfloat16 [1024, 2048], P('sp'), may hold values from -120 to 120, as said below
- cond_vec: float32 [2048], replicated, may hold values from -6 to 6
- ctx_vec: float32 [2048], replicated, may hold values from -6 to 6
- shift_w: bfloat16 [2048, 2048], P('sp', 'tp'), may hold values from -0.125 to 0.125
- scale_w: bfloat16 [2048, 2048], P('sp', 'tp'), may hold values from -0.125 to 0.125
- modgate_w: bfloat16 [2048, 2048], P('sp', 'tp'), may hold values from -0.125 to 0.125
- query_down_weight: bfloat16 [2048, 512], replicated, may hold values from -0.125 to 0.125
- latent_down_weight: bfloat16 [2048, 256], replicated, may hold values from -0.125 to 0.125
- rot_down: bfloat16 [2048, 32], replicated, may hold values from -0.125 to 0.125
- gate_w: bfloat16 [2048, 2048], P(None, 'tp'), may hold values from -0.125 to 0.125
- query_norm_gain: float32 [512], replicated, may hold values from 0.1 to 1.9
- latent_norm_gain: float32 [256], replicated, may hold values from 0.1 to 1.9
- query_plain_weight: bfloat16 [512, 2048], P(None, 'tp'), may hold values from -0.25 to 0.25
- query_rotary_weight: bfloat16 [512, 1024], P(None, 'tp'), may hold values from -0.25 to 0.25
- key_expand_weight: bfloat16 [256, 2048], P(None, 'tp'), may hold values from -0.375 to 0.375
- value_expand_weight: bfloat16 [256, 2048], P(None, 'tp'), may hold values from -0.375 to 0.375
- out_w: bfloat16 [2048, 2048], P('tp'), may hold values from -0.5 to 0.5
- norm_gain: float32 [2048], replicated, may hold values from 0.1 to 1.9
- norm_bias: float32 [2048], replicated, may hold values from -3 to 3
Outputs:
- mixed_out: bfloat16 [2560, 2048], P(('sp', 'tp'))
Inputs may be any that keep to these rules, and one draw needn't show every extreme that they name: `latents`: latent rows are noise plus three slow waves along the whole sequence. Most context rows have their own scales of 1 to 3; a few rows may be far larger.
All inputs are finite; a program needn't handle non-finite values.
Results may differ from a plain program's by a relative error of at most 0.024.
The roundings to bfloat16 on the way count: a program that leaves them out, or rounds other values in their place, can miss the bound.
Values may be sent and summed in bfloat16 or wider, within the bound.
No kernel may reach another device: no remote copies, remote signals or barrier semaphores. Data moves between devices by JAX's collectives and lax.ppermute only.
A program may use at most 128 MiB of HBM per device.

v0:
```python
import jax
import jax.numpy as jnp
from jax import lax
from jax.sharding import PartitionSpec as P

PLAIN_HEAD_SIZE = 64
ROTARY_SIZE = 32
VALUE_HEAD_SIZE = 64
GRID_W = 64


rope_base = 10000.0
norm_floor = 1e-06
residual_weight = 2.0**0.5
score_floor = -1e30


def rms_scale(values, gain):
    return values * lax.rsqrt(jnp.mean(values * values, axis=-1, keepdims=True) + norm_floor) * gain


def rotate(values, positions):
    pair_count = ROTARY_SIZE // 4
    inverse = rope_base ** (-jnp.arange(pair_count, dtype=jnp.float32) / pair_count)
    grid_row = (positions // GRID_W).astype(jnp.float32)
    grid_col = (positions % GRID_W).astype(jnp.float32)
    angles = jnp.stack([grid_row[:, None] * inverse, grid_col[:, None] * inverse], axis=1)
    cosine = jnp.cos(angles)[:, None, :, None, :]
    sine_part = jnp.sin(angles)[:, None, :, None, :]
    shaped = values.reshape(values.shape[0], -1, 2, 2, pair_count)
    first_part = shaped[:, :, :, 0:1, :]
    second = shaped[:, :, :, 1:2, :]
    turned = jnp.concatenate(
        [first_part * cosine - second * sine_part, second * cosine + first_part * sine_part], axis=3
    )
    return turned.reshape(values.shape)


def project(rows, weight):
    return jnp.dot(rows, weight, preferred_element_type=jnp.float32)


def per_device(
    latents,
    context,
    cond_vec,
    ctx_vec,
    shift_w,
    scale_w,
    modgate_w,
    query_down_weight,
    latent_down_weight,
    rot_down,
    gate_w,
    query_norm_gain,
    latent_norm_gain,
    query_plain_weight,
    query_rotary_weight,
    key_expand_weight,
    value_expand_weight,
    out_w,
    norm_gain,
    norm_bias,
):
    width_tp = lax.axis_size("tp")
    block_rows = latents.shape[0]
    seq_rows = block_rows * width_tp
    slab_rows = shift_w.shape[0]
    sp_index = lax.axis_index("sp")
    cond_rows = jnp.stack([jax.nn.silu(cond_vec), jax.nn.silu(ctx_vec)]).astype(jnp.bfloat16)
    cond_here = lax.dynamic_slice_in_dim(cond_rows, sp_index * slab_rows, slab_rows, 1)
    shift_part = project(cond_here, shift_w)
    scale_part = project(cond_here, scale_w)
    gate_part = project(cond_here, modgate_w)
    columns = shift_w.shape[1]
    corner = (jnp.int32(0), lax.axis_index("tp") * columns)
    blank_rows = jnp.zeros((2, latents.shape[1]), jnp.float32)
    shift_vec, scale_vec, gate_vec = lax.psum(
        (
            lax.dynamic_update_slice(blank_rows, shift_part, corner),
            lax.dynamic_update_slice(blank_rows, scale_part, corner),
            lax.dynamic_update_slice(blank_rows, gate_part, corner),
        ),
        ("sp", "tp"),
    )
    latent_in = (latents.astype(jnp.float32) * (1.0 + scale_vec[0]) + shift_vec[0]).astype(
        jnp.bfloat16
    )
    context_in = (context.astype(jnp.float32) * (1.0 + scale_vec[1]) + shift_vec[1]).astype(
        jnp.bfloat16
    )
    heads_here = gate_w.shape[1] // VALUE_HEAD_SIZE
    rows_part = lax.all_gather(latent_in, "tp", axis=0, tiled=True)
    positions = sp_index * seq_rows + jnp.arange(rows_part.shape[0], dtype=jnp.int32)
    q_codes = rms_scale(project(rows_part, query_down_weight), query_norm_gain).astype(jnp.bfloat16)
    kv_codes = rms_scale(project(rows_part, latent_down_weight), latent_norm_gain).astype(
        jnp.bfloat16
    )
    key_rot = rotate(project(rows_part, rot_down), positions).astype(jnp.bfloat16)
    gate_act = project(rows_part, gate_w).astype(jnp.bfloat16)
    project_q_cont = project(q_codes, query_plain_weight).astype(jnp.bfloat16)
    project_q_rot = rotate(project(q_codes, query_rotary_weight), positions).astype(jnp.bfloat16)
    joined = jnp.concatenate([project_q_cont, project_q_rot, gate_act, kv_codes, key_rot], axis=1)
    edge_one = query_plain_weight.shape[1]
    edge_two = edge_one + query_rotary_weight.shape[1]
    edge_three = edge_two + gate_w.shape[1]
    edge_four = edge_three + latent_down_weight.shape[1]
    q_cont = joined[:, :edge_one].reshape(seq_rows, heads_here, PLAIN_HEAD_SIZE)
    q_rot = joined[:, edge_one:edge_two].reshape(seq_rows, heads_here, ROTARY_SIZE)
    gate_act = joined[:, edge_two:edge_three]
    kv_codes = joined[:, edge_three:edge_four]
    key_rot = joined[:, edge_four:]
    ctx_codes = rms_scale(project(context_in, latent_down_weight), latent_norm_gain).astype(
        jnp.bfloat16
    )
    ctx_rot = project(context_in, rot_down).astype(jnp.bfloat16)
    score_scale = (PLAIN_HEAD_SIZE + ROTARY_SIZE) ** (-0.5)

    def expand(codes):
        return (
            project(codes, key_expand_weight).astype(jnp.bfloat16),
            project(codes, value_expand_weight).astype(jnp.bfloat16),
        )

    def attend(running, key_block, value_block, rotary):
        row_top, row_total, weighted = running
        key_count = key_block.shape[0]
        scores = jnp.einsum(
            "qhd,khd->hqk",
            q_cont,
            key_block.reshape(key_count, heads_here, PLAIN_HEAD_SIZE),
            preferred_element_type=jnp.float32,
        )
        scores = (
            scores + jnp.einsum("qhd,kd->hqk", q_rot, rotary, preferred_element_type=jnp.float32)
        ) * score_scale
        new_top = jnp.maximum(row_top, jnp.max(scores, axis=-1))
        weights = jnp.exp(scores - new_top[:, :, None])
        factor = jnp.exp(row_top - new_top)
        row_total = row_total * factor + jnp.sum(weights, axis=-1)
        weighted = weighted * factor[:, :, None] + jnp.einsum(
            "hqk,khd->hqd",
            weights.astype(jnp.bfloat16),
            value_block.reshape(key_count, heads_here, VALUE_HEAD_SIZE),
            preferred_element_type=jnp.float32,
        )
        return (new_top, row_total, weighted)

    start_state = (
        jnp.full((heads_here, seq_rows), score_floor, jnp.float32),
        jnp.zeros((heads_here, seq_rows), jnp.float32),
        jnp.zeros((heads_here, seq_rows, VALUE_HEAD_SIZE), jnp.float32),
    )
    ctx_all_codes, ctx_all_rot = (
        lax.all_gather(ctx_codes, "sp", axis=0, tiled=True),
        lax.all_gather(ctx_rot, "sp", axis=0, tiled=True),
    )
    ctx_keys, ctx_values = expand(ctx_all_codes)
    running = attend(start_state, ctx_keys, ctx_values, ctx_all_rot)
    pieces = (
        lax.all_gather(kv_codes, "sp", axis=0, tiled=True),
        lax.all_gather(key_rot, "sp", axis=0, tiled=True),
    )
    total_rows = pieces[0].shape[0]
    unit_count = total_rows // seq_rows
    grouped = max(
        [1]
        + [
            divisor
            for divisor in range(1, unit_count + 1)
            if unit_count % divisor == 0 and divisor * seq_rows <= 1024
        ]
    )
    blocked = tuple(
        (
            member.reshape(unit_count // grouped, grouped * seq_rows, member.shape[1])
            for member in pieces
        )
    )

    def one_block(carried, members):
        key_block, value_block = expand(members[0])
        return (attend(carried, key_block, value_block, members[1]), None)

    result, unused = lax.scan(one_block, running, blocked)
    running = result
    row_top, row_total, weighted = running
    attended = jnp.transpose(weighted / row_total[:, :, None], (1, 0, 2)).reshape(
        seq_rows, heads_here * VALUE_HEAD_SIZE
    )
    gated = (attended * jax.nn.silu(gate_act.astype(jnp.float32))).astype(jnp.bfloat16)
    branch = lax.psum_scatter(
        project(gated, out_w).astype(jnp.bfloat16), "tp", scatter_dimension=0, tiled=True
    ).astype(jnp.float32)
    blended = residual_weight * latents.astype(jnp.float32) + gate_vec[0] * branch
    row_mean = jnp.mean(blended, axis=-1, keepdims=True)
    centred = blended - row_mean
    row_var = jnp.mean(centred * centred, axis=-1, keepdims=True)
    return (centred * lax.rsqrt(row_var + norm_floor) * norm_gain + norm_bias).astype(jnp.bfloat16)


def solution(mesh):
    in_specs = (
        P(("sp", "tp"), None),
        P("sp", None),
        P(),
        P(),
        P("sp", "tp"),
        P("sp", "tp"),
        P("sp", "tp"),
        P(),
        P(),
        P(),
        P(None, "tp"),
        P(),
        P(),
        P(None, "tp"),
        P(None, "tp"),
        P(None, "tp"),
        P(None, "tp"),
        P("tp", None),
        P(),
        P(),
    )
    out_specs = P(("sp", "tp"), None)
    return jax.shard_map(
        per_device, mesh=mesh, in_specs=in_specs, out_specs=out_specs, check_vma=False
    )
```

profile of v0, /device:TPU:0, one launch (start us, length us, event | category | flops | bytes accessed | tf_op | source)
XLA Modules:
  0.0 249.4 jit_solution(9773118889546091030)
XLA Ops:
  6.6 0.9 multiply_convert_fusion.5
  7.4 0.7 multiply_convert_fusion.4
  8.2 1.2 convolution_dynamic-update-slice_fusion
  9.3 1.1 convolution_dynamic-update-slice_fusion.1
  10.5 1.2 convolution_dynamic-update-slice_fusion.2
  11.7 42.5 %all-reduce = (f32[2,2048]{1,0:T(2,128)S(1)}, f32[2,2048]{1,0:T(2,128)S(1)}, f32[2,2048]{1,0:T(2,128)S(1)}) all-reduce(f32[2,2048]{1,0:T(2,128)S(1)} %convolution_dynamic-update-slice_fusion, f32[2,2048]{1,0:T(2,128)S(1)} %convolution_dynamic-update-slice_fusion.1, ...), channel_id=1, replica_groups=mesh['sp'=8,'tp'=4] {'sp','tp'}, use_global_device_ids=true, to_apply=%region_2.3 | all-reduce | flops 12288 | bytes 98304 | tf_op jit(solution)/shard_map/psum | solution.py:78
  54.2 1.8 fusion.30
  56.1 1.4 convolution_convert_fusion.7
  57.4 26.1 %all_gather.17 = bf16[1024,32]{0,1:T(8,128)(2,1)S(1)} all-gather(bf16[128,32]{0,1:T(8,128)(2,1)S(1)} %convolution_convert_fusion.7), channel_id=1, replica_groups=mesh['sp'=8,'tp'=4] {'sp'}, dimensions={0}, use_global_device_ids=true | all-gather | bytes 73728 | tf_op jit(solution)/shard_map/all_gather | solution.py:156
  83.5 0.1 fusion.40
  83.6 0.1 fusion.39
  83.7 1.6 multiply_reduce_fusion.3
  85.3 0.1 multiply_convert_fusion.3
  85.4 31.5 %all_gather.16 = bf16[1024,256]{1,0:T(8,128)(2,1)S(1)} all-gather(bf16[128,256]{1,0:T(8,128)(2,1)S(1)} %multiply_convert_fusion.3), channel_id=1, replica_groups=mesh['sp'=8,'tp'=4] {'sp'}, dimensions={0}, use_global_device_ids=true | all-gather | bytes 589824 | tf_op jit(solution)/shard_map/all_gather | solution.py:155
  116.9 1.5 convolution_convert_fusion.4
  118.4 1.5 convolution_convert_fusion.3
  119.9 3.0 %multiply_reduce_fusion.1 = (f32[320]{0:T(512)S(1)}, f32[320,512]{1,0:T(8,128)S(1)}) fusion(bf16[320,2048]{1,0:T(8,128)(2,1)} %all-gather.4.cloned.1.call-done, bf16[2048,512]{1,0:T(8,128)(2,1)} %param.29), kind=kOutput, calls=%fused_computation.49 | convolution fusion | flops 671416000 | bytes 4064512 | tf_op jit(solution)/shard_map/dot_general | solution.py:40
  122.9 0.4 fusion.53
  123.3 0.4 convolution_convert_fusion.6
  123.7 0.2 copy.36
  123.9 2.2 multiply_reduce_fusion.2
  126.1 0.8 multiply_convert_fusion.2
  127.0 1.8 fusion.58
  128.8 0.1 subtract_convert_fusion.1
  129.0 31.2 %all-gather = bf16[8,320,32]{1,2,0:T(8,128)(2,1)S(1)} all-gather(bf16[1,320,32]{1,2,0:T(8,128)(2,1)S(1)} %bitcast.115), channel_id=1, replica_groups=mesh['sp'=8,'tp'=4] {'sp'}, dimensions={0}, use_global_device_ids=true | all-gather | bytes 184320 | tf_op jit(solution)/shard_map/all_gather | solution.py:162
  160.2 0.1 copy.38
  160.3 0.2 reshape.332
  160.4 0.7 copy.39
  161.2 1.6 fusion.34
  162.8 1.8 fusion.56
  164.6 2.1 fusion.20
  166.7 2.2 fusion.24
  169.0 37.6 %while.14 = (s32[]{:T(128)}, f32[8,320]{1,0:T(8,128)S(1)}, f32[8,320]{1,0:T(8,128)S(1)}, f32[8,320,64]{1,2,0:T(8,128)S(1)}, bf16[4,640,256]{2,1,0:T(8,128)(2,1)}...) while((s32[]{:T(128)}, f32[8,320]{1,0:T(8,128)S(1)}, ...), condition=%wide.region_11.12_spmd, body=%wide.region_8.11_spmd.sunk | while | flops 872289280 | bytes 39624860 | solution.py:185
  169.0 1.5 convolution_convert_fusion.10
  170.5 1.1 fusion.111
  171.6 2.2 fusion.112
  173.7 1.5 fusion.113
  175.3 1.4 convolution_convert_fusion.11
  176.7 1.7 fusion.114
  178.4 1.5 convolution_convert_fusion.10
  179.9 1.1 fusion.111
  181.0 2.2 fusion.112
  183.1 1.5 fusion.113
  184.7 1.4 convolution_convert_fusion.11
  186.1 1.7 fusion.114
  187.8 1.5 convolution_convert_fusion.10
  189.3 1.1 fusion.111
  190.3 2.2 fusion.112
  192.5 1.5 fusion.113
  194.1 1.4 convolution_convert_fusion.11
  195.5 1.7 fusion.114
  197.2 1.5 convolution_convert_fusion.10
  198.7 1.1 fusion.111
  199.7 2.2 fusion.112
  201.9 1.5 fusion.113
  203.5 1.4 convolution_convert_fusion.11
  204.9 1.7 fusion.114
  206.6 1.0 broadcast_divide_fusion
  207.6 1.4 copy.40
  209.0 4.8 %convolution_convert_fusion.2 = bf16[320,2048]{1,0:T(8,128)(2,1)} fusion(bf16[512,2048]{1,0:T(8,128)(2,1)S(1)} %copy-done, f32[320,512]{1,0:T(8,128)S(1)} %copy.40, bf16[320,2048]{1,0:T(8,128)(2,1)} %all-gather.4.cloned.1.call-done, bf16[2048,512]{1,0:T(8,128)(2,1)} %param.32), kind=kOutput, calls=%fused_computation.28 | convolution fusion | flops 1344143360 | bytes 7471104 | tf_op jit(solution)/shard_map/dot_general | solution.py:40
  213.8 24.7 %reduce-scatter.2.cloned.1.call-done = bf16[80,2048]{1,0:T(8,128)(2,1)} async-done(((bf16[320,2048]{1,0:T(8,128)(2,1)}), bf16[80,2048]{1,0:T(8,128)(2,1)}) %reduce-scatter.2.cloned.1.call-update) | async-done | bytes 327696 | tf_op jit(solution)/shard_map/reduce_scatter | solution.py:192
  238.5 1.2 fusion.31
  239.7 1.2 multiply_reduce_fusion
  241.0 1.9 add_convert_fusion.1
  (75 shorter events, 0.6 us)
Async XLA Ops:
  6.5 202.4 %copy-start = (bf16[512,2048]{1,0:T(8,128)(2,1)S(1)}, bf16[512,2048]{1,0:T(8,128)(2,1)}, u32[]{:S(2)}) copy-start(bf16[512,2048]{1,0:T(8,128)(2,1)} %param.39) | copy-start | bytes 6291460
  6.5 77.2 %copy-start.14 = (bf16[128,2048]{1,0:T(8,128)(2,1)S(1)}, bf16[128,2048]{1,0:T(8,128)(2,1)}, u32[]{:S(2)}) copy-start(bf16[128,2048]{1,0:T(8,128)(2,1)} %param.23) | copy-start | bytes 1572868
  6.5 78.8 %copy-start.13 = (f32[256]{0:T(256)S(1)}, f32[256]{0:T(256)}, u32[]{:S(2)}) copy-start(f32[256]{0:T(256)} %param.34) | copy-start | bytes 3076
  6.5 113.3 %all-gather.4.cloned.1.call-start = ((), (), s32[]{:S(2)}) async-start(), calls=%async_computation.1 | async-start | bytes 1638400 | tf_op jit(solution)/shard_map/all_gather | solution.py:93
  10.5 106.4 %copy-start.1 = (bf16[256,512]{1,0:T(8,128)(2,1)S(1)}, bf16[256,512]{1,0:T(8,128)(2,1)}, u32[]{:S(2)}) copy-start(bf16[256,512]{1,0:T(8,128)(2,1)} %param.37) | copy-start | bytes 786436
  56.0 113.0 %all-gather.6.cloned.1.call-start = ((), (), s32[]{:S(2)}) async-start(), calls=%async_computation.2 | async-start | bytes 1474560 | tf_op jit(solution)/shard_map/all_gather | solution.py:161
  56.1 62.3 %copy-start.2 = (bf16[256,512]{1,0:T(8,128)(2,1)S(1)}, bf16[256,512]{1,0:T(8,128)(2,1)}, u32[]{:S(2)}) copy-start(bf16[256,512]{1,0:T(8,128)(2,1)} %param.38) | copy-start | bytes 786436
  119.9 3.0 %copy-start.8 = (bf16[512,256]{1,0:T(8,128)(2,1)S(1)}, bf16[512,256]{1,0:T(8,128)(2,1)}, u32[]{:S(2)}) copy-start(bf16[512,256]{1,0:T(8,128)(2,1)} %param.36) | copy-start | bytes 786436
  119.9 3.0 %copy-start.12 = (f32[512]{0:T(512)S(1)}, f32[512]{0:T(512)}, u32[]{:S(2)}) copy-start(f32[512]{0:T(512)} %param.33) | copy-start | bytes 6148
  119.9 3.4 %copy-start.7 = (bf16[512,512]{1,0:T(8,128)(2,1)S(1)}, bf16[512,512]{1,0:T(8,128)(2,1)}, u32[]{:S(2)}) copy-start(bf16[512,512]{1,0:T(8,128)(2,1)} %param.35) | copy-start | bytes 1572868
  123.7 3.3 %copy-start.9 = (bf16[2048,32]{0,1:T(8,128)(2,1)S(1)}, bf16[2048,32]{0,1:T(8,128)(2,1)}, u32[]{:S(2)}) copy-start(bf16[2048,32]{0,1:T(8,128)(2,1)} %param.31) | copy-start | bytes 393220
  127.0 111.5 %reduce-scatter.2.cloned.1.call-start = ((), (), s32[]{:S(2)}) async-start(), calls=%async_computation.3 | async-start | bytes 1638400 | tf_op jit(solution)/shard_map/reduce_scatter | solution.py:192
  161.2 1.6 copy-start.5
  164.6 2.2 copy-start.6
  173.7 1.6 copy-start.3
  183.1 1.6 copy-start.3
  192.5 1.6 copy-start.3
  201.9 1.6 copy-start.3
  209.0 29.5 %copy-start.4 = (bf16[80,2048]{1,0:T(8,128)(2,1)S(1)}, bf16[80,2048]{1,0:T(8,128)(2,1)}, u32[]{:S(2)}) copy-start(bf16[80,2048]{1,0:T(8,128)(2,1)} %param.22) | copy-start | bytes 983044
  213.8 27.2 %copy-start.10 = (f32[2048]{0:T(1024)S(1)}, f32[2048]{0:T(1024)}, u32[]{:S(2)}) copy-start(f32[2048]{0:T(1024)} %param.41) | copy-start | bytes 24580
  213.8 27.2 %copy-start.11 = (f32[2048]{0:T(1024)S(1)}, f32[2048]{0:T(1024)}, u32[]{:S(2)}) copy-start(f32[2048]{0:T(1024)} %param.40) | copy-start | bytes 24580
Sparse Core Ops, SparseCore 0:
  56.1 17.9 all-gather.3
  127.1 40.2 all-gather.5
  213.9 24.5 reduce-scatter.1
where the time goes:
time: 251 us; the launch traced here: 249 us
  blocking collectives  131 us (52%)
  matrix products  58.6 us (23%)
  waiting for transfers between devices  24.7 us (10%)
  other arithmetic  18.4 us (7%)
  between operations  13.5 us (5%)
  local copies, waits for them, and re-layouts  2.64 us (1%)
    psum x1, blocking collectives, per_device(): lax.psum((lax.dynamic_update_slice(blank_rows, shift_part, corner), lax.d...  42.5 us
    dot_general x21, matrix products, project(): return jnp.dot(rows, weight, preferred_element_type=jnp.float32)  33.4 us
    all_gather x1, blocking collectives, per_device(): lax.all_gather(ctx_codes, 'sp', axis=0, tiled=True)  31.5 us
    all_gather x1, blocking collectives, per_device(): lax.all_gather(key_rot, 'sp', axis=0, tiled=True)  31.2 us
    all_gather x1, blocking collectives, per_device(): lax.all_gather(ctx_rot, 'sp', axis=0, tiled=True)  26.1 us
    reduce_scatter x1, waiting for transfers between devices, per_device(): lax.psum_scatter(project(gated, out_w).astype(jnp.bfloat16), 'tp', scatte...  24.7 us
    dot_general x5, matrix products, attend(): jnp.einsum('qhd,kd->hqk', q_rot, rotary, preferred_element_type=jnp.float32)  10.2 us
    dot_general x5, matrix products, attend(): jnp.einsum('hqk,khd->hqd', weights.astype(jnp.bfloat16), value_block.resh...  8.97 us
  transfers between devices with their start and end apart: 3, of which 1 were waited for; matrix products, arithmetic and copies ran while one was open for 7% of the time, Pallas kernels for 0%

commit v1 on v0

v1 whole, which is shorter than its diff:
```python
import math

import jax
import jax.numpy as jnp
from jax import lax
from jax.experimental import pallas as pl
from jax.experimental.pallas import tpu as pltpu
from jax.sharding import PartitionSpec as P

PLAIN = 64
ROT = 32
VALUE = 64
GRID_W = 64
LANES = 128
GROUP = 16
ROPE_BASE = 10000.0
FLOOR = 1e-06
RESIDUAL = 2.0**0.5
NEG = -1e30

VMEM = pl.BlockSpec(memory_space=pltpu.VMEM)
SMEM = pl.BlockSpec(memory_space=pltpu.SMEM)
PARAMS = pltpu.CompilerParams(vmem_limit_bytes=56 * 2**20)


def dot(a, b):
    return lax.dot_general(a, b, (((1,), (0,)), ((), ())), preferred_element_type=jnp.float32)


def dot_t(a, b):
    return lax.dot_general(a, b, (((1,), (1,)), ((), ())), preferred_element_type=jnp.float32)


def round_up(value, step):
    return -(-value // step) * step


def cost(flops, moved):
    return pl.CostEstimate(flops=flops, transcendentals=0, bytes_accessed=moved)


def lane_index(shape):
    return lax.broadcasted_iota(jnp.int32, shape, len(shape) - 1)


def turn(values, cosine, sine):
    width = values.shape[1]
    upper = pltpu.roll(values, width - 8, 1)
    lower = pltpu.roll(values, 8, 1)
    swapped = jnp.where((lane_index(values.shape) & 8) == 0, upper, lower)
    return values * cosine + swapped * sine


def rms(values, gain):
    return values * lax.rsqrt(jnp.mean(values * values, axis=-1, keepdims=True) + FLOOR) * gain


def mod_kernel(cond_ref, shift_ref, scale_ref, gate_ref, out_ref):
    rows = cond_ref[...]
    rows = (rows * (1.0 / (1.0 + jnp.exp(-rows)))).astype(jnp.bfloat16)
    out_ref[0:2, :] = dot(rows, shift_ref[...])[0:2, :]
    out_ref[2:4, :] = dot(rows, scale_ref[...])[0:2, :]
    out_ref[4:6, :] = dot(rows, gate_ref[...])[0:2, :]
    out_ref[6:8, :] = jnp.zeros((2, out_ref.shape[1]), jnp.float32)


def fill_mod(me_ref, pieces_ref, mod_ref, xors):
    width = pieces_ref.shape[-1]
    for place, xor in enumerate(xors):
        column = pl.multiple_of((me_ref[0] ^ xor) * width, LANES)
        mod_ref[:, pl.ds(column, width)] = pieces_ref[place]


def codes_kernel(xors, me_ref, mod_ref, lat_ref, ctx_ref, w_ref, gain_ref, cos_ref, sin_ref, out_ref, vec_ref, rows_ref):
    fill_mod(me_ref, mod_ref, vec_ref, xors)
    lat_rows, ctx_rows = lat_ref.shape[0], ctx_ref.shape[0]
    unit = rows_ref.shape[0]
    latent = gain_ref.shape[1]
    rows_ref[0:lat_rows, :] = lat_ref[...].astype(jnp.float32) * (1.0 + vec_ref[2:3, :]) + vec_ref[0:1, :]
    rows_ref[lat_rows : lat_rows + ctx_rows, :] = ctx_ref[...].astype(jnp.float32) * (1.0 + vec_ref[3:4, :]) + vec_ref[1:2, :]
    if lat_rows + ctx_rows < unit:
        rows_ref[lat_rows + ctx_rows :, :] = jnp.zeros((unit - lat_rows - ctx_rows, rows_ref.shape[1]), jnp.float32)
    both = dot(rows_ref[...].astype(jnp.bfloat16), w_ref[...])
    out_ref[0:unit, :] = rms(both[:, :latent], gain_ref[...]).astype(jnp.bfloat16)
    turned = turn(both[:, latent:], cos_ref[...], sin_ref[...])
    lanes = lane_index((GROUP, LANES))
    tiles = []
    for tile in range(latent // LANES):
        packed = jnp.zeros((GROUP, LANES), jnp.float32)
        for slot in range(LANES // ROT):
            group = tile * (LANES // ROT) + slot
            if group * GROUP < unit:
                piece = turned[group * GROUP : (group + 1) * GROUP, :]
                if slot:
                    piece = pltpu.roll(piece, slot * ROT, 1)
                packed = jnp.where((lanes // ROT) == slot, piece, packed)
        tiles.append(packed)
    out_ref[unit:, :] = jnp.concatenate(tiles, axis=1).astype(jnp.bfloat16)


def modulate_blocks(vec_ref, blocks, rows_ref):
    count = blocks[0].shape[0]
    for place, block in enumerate(blocks):
        rows_ref[place * count : (place + 1) * count, :] = block[...].astype(jnp.float32) * (1.0 + vec_ref[2:3, :]) + vec_ref[0:1, :]


def query_kernel(xors, *refs):
    n = len(xors)
    me_ref, mod_ref = refs[:2]
    blocks = refs[2 : 2 + n]
    down_ref, gain_ref, plain_ref, rotary_ref, cos_ref, sin_ref, out_ref, vec_ref, rows_ref = refs[2 + n :]
    fill_mod(me_ref, mod_ref, vec_ref, xors)
    modulate_blocks(vec_ref, blocks, rows_ref)
    codes = rms(dot(rows_ref[...].astype(jnp.bfloat16), down_ref[...]), gain_ref[...]).astype(jnp.bfloat16)
    content = dot(codes, plain_ref[...])
    rotary = dot(codes, rotary_ref[...])
    heads = out_ref.shape[0]
    lanes = lane_index((content.shape[0], LANES))
    per_tile = LANES // ROT
    for tile in range(heads // per_tile):
        turned = turn(rotary[:, tile * LANES : (tile + 1) * LANES], cos_ref[...], sin_ref[...])
        for slot in range(per_tile):
            head = tile * per_tile + slot
            pair = content[:, (head // 2) * LANES : (head // 2 + 1) * LANES]
            goal = PLAIN if head % 2 == 0 else 0
            shift = (goal - slot * ROT) % LANES
            moved = pltpu.roll(turned, shift, 1) if shift else turned
            if head % 2 == 0:
                joined = jnp.where(lanes < PLAIN, pair, jnp.where(lanes < PLAIN + ROT, moved, 0.0))
            else:
                joined = jnp.where(lanes >= PLAIN, pair, jnp.where(lanes < ROT, moved, 0.0))
            out_ref[head] = joined.astype(jnp.bfloat16)


def gate_kernel(xors, *refs):
    n = len(xors)
    me_ref, mod_ref = refs[:2]
    blocks = refs[2 : 2 + n]
    w_ref, out_ref, vec_ref, rows_ref = refs[2 + n :]
    fill_mod(me_ref, mod_ref, vec_ref, xors)
    modulate_blocks(vec_ref, blocks, rows_ref)
    out_ref[...] = dot(rows_ref[...].astype(jnp.bfloat16), w_ref[...]).astype(jnp.bfloat16)


def attend_kernel(n_kv, unit, valid, first, last, *refs):
    q_ref = refs[0]
    kv_refs = refs[1 : 1 + n_kv]
    at = 1 + n_kv
    key_w_ref, value_w_ref = refs[at : at + 2]
    at += 2
    if not first:
        state_ref = refs[at]
        at += 1
    if last:
        gate_ref = refs[at]
        at += 1
        keep_ref, send_ref = refs[at : at + 2]
        at += 2
    else:
        new_ref = refs[at]
        at += 1
    rot_ref, key_ref, val_ref = refs[at : at + 3]
    factor = (PLAIN + ROT) ** (-0.5) * math.log2(math.e)
    groups = unit // GROUP
    rows = [ref.shape[0] * unit for ref in kv_refs]
    starts = [sum(rows[:i]) for i in range(n_kv)]
    total = sum(rows)

    @pl.when(pl.program_id(0) == 0)
    def _():
        lanes = lane_index((GROUP, LANES))
        for ref, start in zip(kv_refs, starts):
            for index in range(ref.shape[0]):
                packed = ref[index, unit:, :].astype(jnp.float32)
                for group in range(groups):
                    tile, slot = group // (LANES // ROT), group % (LANES // ROT)
                    part = packed[:, tile * LANES : (tile + 1) * LANES]
                    low = pltpu.roll(part, (-slot * ROT) % LANES, 1) if slot else part
                    high = pltpu.roll(part, (PLAIN - slot * ROT) % LANES, 1)
                    both = jnp.where(lanes < ROT, low, jnp.where((lanes >= PLAIN) & (lanes < PLAIN + ROT), high, 0.0))
                    at_row = start + index * unit + group * GROUP
                    rot_ref[at_row : at_row + GROUP, :] = both.astype(jnp.bfloat16)

    weights = jnp.concatenate([key_w_ref[...], value_w_ref[...]], axis=1)
    for ref, start, count in zip(kv_refs, starts, rows):
        codes = ref[:, :unit, :].reshape(count, ref.shape[2])
        both = dot(codes, weights).astype(jnp.bfloat16)
        key_ref[start : start + count, :] = both[:, :LANES]
        val_ref[start : start + count, :] = both[:, LANES:]
    lanes = lane_index((total, LANES))
    queries = q_ref.shape[1]
    out_lanes = lane_index((queries, LANES))
    halves = []
    for head in range(2):
        own = (lanes < PLAIN) if head == 0 else (lanes >= PLAIN)
        k_full = jnp.where(own, key_ref[...], rot_ref[...])
        ones = (lanes == (PLAIN if head == 0 else 0)).astype(jnp.bfloat16)
        v_full = jnp.where(own, val_ref[...], ones)
        sum_lane = PLAIN if head == 0 else 0
        scores = dot_t(q_ref[head], k_full)
        if valid < unit:
            spot = lax.broadcasted_iota(jnp.int32, scores.shape, 1) % unit
            scores = jnp.where(spot < valid, scores, NEG)
        top = jnp.max(scores, axis=1, keepdims=True)
        if not first:
            before = state_ref[head]
            old_top = before[:, sum_lane + 1 : sum_lane + 2]
            top = jnp.maximum(top, old_top)
        probs = jnp.exp2((scores - top) * factor).astype(jnp.bfloat16)
        out = dot(probs, v_full)
        if not first:
            out = out + before * jnp.exp2((old_top - top) * factor)
        if last:
            halves.append(out * (1.0 / out[:, sum_lane : sum_lane + 1]))
        else:
            new_ref[head] = jnp.where(out_lanes == sum_lane + 1, top, out)
    if last:
        attended = jnp.where(out_lanes < PLAIN, halves[0], halves[1])
        gate = gate_ref[...].astype(jnp.float32)
        gated = (attended * (gate * (1.0 / (1.0 + jnp.exp(-gate))))).astype(jnp.bfloat16)
        keep_ref[...] = gated[: queries // 2]
        send_ref[...] = gated[queries // 2 :]


def attend(q_full, kv, key_w, value_w, state, gate, unit, valid):
    heads, queries, _ = q_full.shape
    first, last = state is None, gate is not None
    total = sum(part.shape[0] for part in kv) * unit
    whole = lambda part: pl.BlockSpec(part.shape, lambda g: (0,) * part.ndim)
    column = lambda count: pl.BlockSpec((count, LANES), lambda g: (0, g))
    heads_spec = pl.BlockSpec((2, queries, LANES), lambda g: (g, 0, 0))
    in_specs = [heads_spec] + [whole(part) for part in kv] + [column(key_w.shape[0])] * 2
    args = [q_full, *kv, key_w, value_w]
    if not first:
        in_specs.append(heads_spec)
        args.append(state)
    if last:
        in_specs.append(column(queries))
        args.append(gate)
        out_specs = [column(queries // 2)] * 2
        out_shape = [jax.ShapeDtypeStruct((queries // 2, heads * VALUE), jnp.bfloat16)] * 2
    else:
        out_specs = heads_spec
        out_shape = jax.ShapeDtypeStruct((heads, queries, LANES), jnp.float32)
    return pl.pallas_call(
        lambda *refs: attend_kernel(len(kv), unit, valid, first, last, *refs),
        grid=(heads // 2,),
        in_specs=in_specs,
        out_specs=out_specs,
        out_shape=out_shape,
        scratch_shapes=[pltpu.VMEM((total, LANES), jnp.bfloat16)] * 3,
        compiler_params=PARAMS,
        cost_estimate=cost(4 * heads * queries * total * LANES, 2**20),
        name="attend",
    )(*args)


def branch_kernel(mine_ref, theirs_ref, w_mine_ref, w_theirs_ref, far_ref, near_ref):
    near = near_ref.shape[0]
    far_ref[...] = (
        dot(mine_ref[near:, :], w_mine_ref[...]) + dot(theirs_ref[near:, :], w_theirs_ref[...])
    ).astype(jnp.bfloat16)
    near_ref[...] = dot(mine_ref[:near, :], w_mine_ref[...]) + dot(theirs_ref[:near, :], w_theirs_ref[...])


def norm_kernel(xors, me_ref, mod_ref, lat_ref, near_ref, far_ref, gain_ref, bias_ref, out_ref, vec_ref):
    fill_mod(me_ref, mod_ref, vec_ref, xors)
    branch = near_ref[...] + far_ref[...].astype(jnp.float32)
    blended = RESIDUAL * lat_ref[...].astype(jnp.float32) + vec_ref[4:5, :] * branch
    centred = blended - jnp.mean(blended, axis=-1, keepdims=True)
    variance = jnp.mean(centred * centred, axis=-1, keepdims=True)
    out_ref[...] = (centred * lax.rsqrt(variance + FLOOR) * gain_ref[...] + bias_ref[...]).astype(jnp.bfloat16)


def call(kernel, out_shape, args, scratch=(), flops=0, moved=0, smem=0, name=None):
    return pl.pallas_call(
        kernel,
        in_specs=[SMEM] * smem + [VMEM] * (len(args) - smem),
        out_specs=jax.tree.map(lambda _: VMEM, out_shape),
        out_shape=out_shape,
        scratch_shapes=list(scratch),
        compiler_params=PARAMS,
        cost_estimate=cost(flops, moved),
        name=name,
    )(*args)


def angle_tables(positions, rotated):
    lane = jnp.arange(LANES, dtype=jnp.int32)
    inverse = ROPE_BASE ** (-(lane % 8).astype(jnp.float32) / 8)
    on_column = (lane // 16) % 2 == 1
    place = jnp.where(on_column[None, :], (positions % GRID_W)[:, None], (positions // GRID_W)[:, None])
    angles = place.astype(jnp.float32) * inverse[None, :]
    sign = jnp.where((lane // 8) % 2 == 0, -1.0, 1.0)[None, :]
    cosine = jnp.where(rotated[:, None], jnp.cos(angles), 1.0)
    sine = jnp.where(rotated[:, None], jnp.sin(angles) * sign, 0.0)
    return cosine, sine


def per_device(
    latents,
    context,
    cond_vec,
    ctx_vec,
    shift_w,
    scale_w,
    modgate_w,
    query_down_weight,
    latent_down_weight,
    rot_down,
    gate_w,
    query_norm_gain,
    latent_norm_gain,
    query_plain_weight,
    query_rotary_weight,
    key_expand_weight,
    value_expand_weight,
    out_w,
    norm_gain,
    norm_bias,
):
    n_tp = lax.axis_size("tp")
    n_sp = lax.axis_size("sp")
    total = n_tp * n_sp
    sp_index, tp_index = lax.axis_index("sp"), lax.axis_index("tp")
    block, width = latents.shape
    f32, bf16 = jnp.float32, jnp.bfloat16

    def swap(array, mask):
        return lax.ppermute(array, ("sp", "tp"), [(i, i ^ mask) for i in range(total)])

    sp_masks = []
    mask = n_sp // 2
    while mask:
        sp_masks.append(mask * n_tp)
        mask //= 2
    tp_masks = []
    mask = n_tp // 2
    while mask:
        tp_masks.append(mask)
        mask //= 2
    me = tp_index.astype(jnp.int32).reshape(1)

    xors, blocks = [0], [latents]
    for mask in tp_masks:
        blocks = blocks + [swap(item, mask) for item in blocks]
        xors = xors + [x ^ mask for x in xors]
    out_w_pair = swap(out_w, 1)

    slab = shift_w.shape[0]
    cond = jnp.stack([cond_vec, ctx_vec])
    cond = lax.dynamic_slice_in_dim(cond, sp_index * slab, slab, 1)
    cond = jnp.concatenate([cond, jnp.zeros((6, slab), f32)], axis=0)
    columns = shift_w.shape[1]
    mod = call(mod_kernel, jax.ShapeDtypeStruct((8, columns), f32), (cond, shift_w, scale_w, modgate_w), name="mod")
    for mask in sp_masks:
        mod = mod + swap(mod, mask)
    mod = mod[None]
    for mask in tp_masks:
        mod = jnp.concatenate([mod, swap(mod, mask)], axis=0)
    vec_scratch = pltpu.VMEM((8, width), f32)

    ctx_rows = context.shape[0] // n_tp
    ctx_here = lax.dynamic_slice_in_dim(context, tp_index * ctx_rows, ctx_rows, 0)
    valid = block + ctx_rows
    unit = round_up(valid, GROUP)
    latent = latent_down_weight.shape[1]
    codes_w = jnp.concatenate([latent_down_weight, rot_down, jnp.zeros((width, LANES - ROT), bf16)], axis=1)
    row = jnp.arange(unit, dtype=jnp.int32)
    unit_cos, unit_sin = angle_tables((sp_index * n_tp + tp_index) * block + row, row < block)
    own = call(
        lambda *refs: codes_kernel(xors, *refs),
        jax.ShapeDtypeStruct((unit + GROUP, latent), bf16),
        (me, mod, latents, ctx_here, codes_w, latent_norm_gain.reshape(1, -1), unit_cos, unit_sin),
        scratch=(vec_scratch, pltpu.VMEM((unit, width), f32)),
        smem=1,
        name="codes",
    )

    near = own[None]
    for mask in sp_masks[:-1] + tp_masks[:-2]:
        near = jnp.concatenate([near, swap(near, mask)], axis=0)
    side_a, side_b = sp_masks[-1], tp_masks[-2]
    half = near.shape[0] // 2
    near_c = swap(near, 1)
    over_a = swap(near, side_a)
    over_b = swap(near, side_b)
    over_a_c = swap(over_a, 1)
    over_b_c = swap(over_b, 1)
    far_a = swap(over_b[:half], side_a)
    far_b = swap(over_a[half:], side_b)
    far_a_c = swap(far_a, 1)
    far_b_c = swap(far_b, 1)

    heads = gate_w.shape[1] // VALUE
    seq = block * n_tp
    order = jnp.concatenate([(tp_index ^ x) * block + jnp.arange(block, dtype=jnp.int32) for x in xors])
    q_cos, q_sin = angle_tables(sp_index * seq + order, jnp.ones((seq,), bool))
    rows_scratch = pltpu.VMEM((seq, width), f32)
    q_full = call(
        lambda *refs: query_kernel(xors, *refs),
        jax.ShapeDtypeStruct((heads, seq, LANES), bf16),
        (me, mod, *blocks, query_down_weight, query_norm_gain.reshape(1, -1), query_plain_weight, query_rotary_weight, q_cos, q_sin),
        scratch=(vec_scratch, rows_scratch),
        smem=1,
        flops=2 * seq * width * query_down_weight.shape[1],
        name="queries",
    )
    gate = call(
        lambda *refs: gate_kernel(xors, *refs),
        jax.ShapeDtypeStruct((seq, gate_w.shape[1]), bf16),
        (me, mod, *blocks, gate_w),
        scratch=(vec_scratch, rows_scratch),
        smem=1,
        flops=2 * seq * width * gate_w.shape[1],
        name="gate",
    )

    step = lambda kv, state, last: attend(
        q_full, kv, key_expand_weight, value_expand_weight, state, gate if last else None, unit, valid
    )
    state = step([near, near_c], None, False)
    state = step([over_a, over_b, over_a_c, over_b_c], state, False)
    keep, send = step([far_a, far_b, far_a_c, far_b_c], state, True)

    theirs = swap(send, 1)
    rows = keep.shape[0] // 2
    far, close = call(
        branch_kernel,
        [jax.ShapeDtypeStruct((rows, width), bf16), jax.ShapeDtypeStruct((keep.shape[0] - rows, width), f32)],
        (keep, theirs, out_w, out_w_pair),
        flops=4 * keep.shape[0] * keep.shape[1] * width,
        name="branch",
    )
    far = swap(far, tp_masks[-2])
    for mask in tp_masks[:-2][::-1]:
        close = close + far.astype(f32)
        rows = close.shape[0] // 2
        far = swap(close[rows:].astype(bf16), mask)
        close = close[:rows]
    return call(
        lambda *refs: norm_kernel(xors, *refs),
        jax.ShapeDtypeStruct((block, width), bf16),
        (me, mod, latents, close, far, norm_gain.reshape(1, -1), norm_bias.reshape(1, -1)),
        scratch=(vec_scratch,),
        smem=1,
        name="norm",
    )


def solution(mesh):
    in_specs = (
        P(("sp", "tp"), None),
        P("sp", None),
        P(),
        P(),
        P("sp", "tp"),
        P("sp", "tp"),
        P("sp", "tp"),
        P(),
        P(),
        P(),
        P(None, "tp"),
        P(),
        P(),
        P(None, "tp"),
        P(None, "tp"),
        P(None, "tp"),
        P(None, "tp"),
        P("tp", None),
        P(),
        P(),
    )
    return jax.shard_map(
        per_device, mesh=mesh, in_specs=in_specs, out_specs=P(("sp", "tp"), None), check_vma=False
    )
```

time: 251 us -> 124 us (0.49)
  blocking collectives: 131 us -> 0 us
  matrix products: 58.6 us -> 0 us
  Pallas kernels: 0 us -> 52.2 us
  starting transfers between devices: 0.09 us -> 18.8 us
  between operations: 13.5 us -> 0.22 us
  other arithmetic: 18.4 us -> 10.2 us
  waiting for transfers between devices: 24.7 us -> 32.8 us
  local copies, waits for them, and re-layouts: 2.64 us -> 9.18 us
    all_gather x3 -> x0, blocking collectives: 88.8 us -> none  [the longest x1 31.5 us: per_device(): lax.all_gather(ctx_codes, 'sp', axis=0, tiled=True)]
    dot_general x36 -> x0, matrix products: 58.6 us -> none  [the longest x21 33.4 us: project(): return jnp.dot(rows, weight, preferred_element_type=jnp.float32)]
    pallas_call x0 -> x9, Pallas kernels: none -> 52.2 us  [the longest x3 31.8 us: attend(): pl.pallas_call(lambda *refs: attend_kernel(len(kv), unit, valid, first, l...]
    psum x1 -> x0, blocking collectives: 42.5 us -> none  [per_device(): lax.psum((lax.dynamic_update_slice(blank_rows, shift_part, corner), lax.d...]
    ppermute x0 -> x22, waiting for transfers between devices: none -> 32.8 us  [swap(): lax.ppermute(array, ('sp', 'tp'), [(i, i ^ mask) for i in range(total)])]
    reduce_scatter x1 -> x0, waiting for transfers between devices: 24.7 us -> none  [per_device(): lax.psum_scatter(project(gated, out_w).astype(jnp.bfloat16), 'tp', scatte...]
    ppermute x0 -> x22, starting transfers between devices: none -> 18.8 us  [swap(): lax.ppermute(array, ('sp', 'tp'), [(i, i ^ mask) for i in range(total)])]
    reduce_sum x7 -> x0, other arithmetic: 10.7 us -> none  [the longest x5 8.22 us: attend(): row_total = row_total * factor + jnp.sum(weights, axis=-1)]
  transfers between devices with their start and end apart: 3 -> 22, of which waited for: 1 -> 11; matrix products, arithmetic and copies ran while one was open for 7% -> 11% of each run, Pallas kernels for 0% -> 35%
where the time goes in v1:
time: 124 us; the launch traced here: 123 us
  Pallas kernels  52.2 us (42%)
  waiting for transfers between devices  32.8 us (26%)
  starting transfers between devices  18.8 us (15%)
  other arithmetic  10.2 us (8%)
  local copies, waits for them, and re-layouts  9.18 us (7%)
    ppermute x22, waiting for transfers between devices, swap(): lax.ppermute(array, ('sp', 'tp'), [(i, i ^ mask) for i in range(total)])  32.8 us
    pallas_call x3, Pallas kernels, attend(): pl.pallas_call(lambda *refs: attend_kernel(len(kv), unit, valid, first, l...  31.8 us
    pallas_call x6, Pallas kernels, call(): pl.pallas_call(kernel, in_specs=[SMEM] * smem + [VMEM] * (len(args) - sme...  20.4 us
    ppermute x22, starting transfers between devices, swap(): lax.ppermute(array, ('sp', 'tp'), [(i, i ^ mask) for i in range(total)])  18.8 us
    unnamed x35, local copies, waits for them, and re-layouts  6 us
    concatenate x1, other arithmetic, per_device(): jnp.concatenate([latent_down_weight, rot_down, jnp.zeros((width, LANES -...  2.76 us
  transfers between devices with their start and end apart: 22, of which 11 were waited for; matrix products, arithmetic and copies ran while one was open for 11% of the time, Pallas kernels for 35%

profile of v1, /device:TPU:0, one launch (start us, length us, event | category | flops | bytes accessed | tf_op | source)
XLA Modules:
  0.0 123.4 jit_solution(16886658814980781598)
XLA Ops:
  0.0 0.8 fusion.1
  0.8 0.6 concatenate.30.cond_ref
  1.4 1.9 %mod.1 = f32[8,512]{1,0:T(8,128)} custom-call(f32[8,256]{1,0:T(8,128)} %concatenate.30.cond_ref, bf16[256,512]{1,0:T(8,128)(2,1)} %shift_ref.1, bf16[256,512]{1,0:T(8,128)(2,1)} %scale_ref.1, bf16[256,512]{1,0:T(8,128)(2,1)} %gate_ref.1), custom_call_target="tpu_custom_call" | custom-call | tf_op jit(solution)/shard_map/mod/pallas_call | solution.py:276
  3.4 4.1 %collective-permute-start = (f32[8,512]{1,0:T(8,128)}, f32[8,512]{1,0:T(8,128)S(1)}, u32[]{:S(2)}, u32[]{:S(2)}) collective-permute-start(f32[8,512]{1,0:T(8,128)} %mod.1), channel_id=1, source_target_pairs={{0,16},{1,17},{2,18},{3,19},{4,20},{5,21},{6,22},{7,23},{8,24},{9,... | collective-permute-start | bytes 49160 | tf_op jit(solution)/shard_map/ppermute | solution.py:330
  7.4 1.2 copy.21
  8.6 0.1 pad.8.clone
  8.7 0.7 constant_dynamic-slice_fusion.refs_3_
  9.4 2.8 %maximum_maximum_fusion.refs_4_ = bf16[2048,384]{1,0:T(8,128)(2,1)} fusion(bf16[2048,32]{1,0:T(8,128)(2,1)S(1)} %copy.21, bf16[2048,256]{1,0:T(8,128)(2,1)} %param.28, bf16[384]{0:T(512)(128)(2,1)S(1)} %pad.8.clone), kind=kLoop, calls=%fused_computation | loop fusion | flops 4718592 | bytes 2753280 | tf_op jit(solution)/shard_map/concatenate | solution.py:368
  12.2 1.6 %collective-permute-start.1 = (f32[8,512]{1,0:T(8,128)S(1)}, f32[8,512]{1,0:T(8,128)S(1)}, u32[]{:S(2)}, u32[]{:S(2)}) collective-permute-start(f32[8,512]{1,0:T(8,128)S(1)} %add.157), channel_id=1, source_target_pairs={{0,8},{1,9},{2,10},{3,11},{4,12},{5,13},{6,14},{7,15},{8,0},{9,1},... | collective-permute-start | bytes 49160 | tf_op jit(solution)/shard_map/ppermute | solution.py:330
  13.9 2.1 %collective-permute-done.1 = f32[8,512]{1,0:T(8,128)S(1)} collective-permute-done((f32[8,512]{1,0:T(8,128)S(1)}, f32[8,512]{1,0:T(8,128)S(1)}, u32[]{:S(2)}, u32[]{:S(2)}) %collective-permute-start.1) | collective-permute-done | bytes 16416 | tf_op jit(solution)/shard_map/ppermute | solution.py:330
  16.0 1.5 %collective-permute-start.2 = (f32[8,512]{1,0:T(8,128)S(1)}, f32[8,512]{1,0:T(8,128)S(1)}, u32[]{:S(2)}, u32[]{:S(2)}) collective-permute-start(f32[8,512]{1,0:T(8,128)S(1)} %add.158), channel_id=1, source_target_pairs={{0,4},{1,5},{2,6},{3,7},{4,0},{5,1},{6,2},{7,3},{8,12},{9,13},{10,... | collective-permute-start | bytes 49160 | tf_op jit(solution)/shard_map/ppermute | solution.py:330
  17.5 2.2 %collective-permute-done.2 = f32[8,512]{1,0:T(8,128)S(1)} collective-permute-done((f32[8,512]{1,0:T(8,128)S(1)}, f32[8,512]{1,0:T(8,128)S(1)}, u32[]{:S(2)}, u32[]{:S(2)}) %collective-permute-start.2) | collective-permute-done | bytes 16416 | tf_op jit(solution)/shard_map/ppermute | solution.py:330
  19.8 1.5 %collective-permute-start.3 = (f32[1,8,512]{2,1,0:T(8,128)S(1)}, f32[1,8,512]{2,1,0:T(8,128)S(1)}, u32[]{:S(2)}, u32[]{:S(2)}) collective-permute-start(f32[1,8,512]{2,1,0:T(8,128)S(1)} %add_bitcast_fusion), channel_id=1, source_target_pairs={{0,2},{1,3},{2,0},{3,1},{4,6},{5,7},{6,4},{7,5},{8,10},{9,11},{10,... | collective-permute-start | bytes 49160 | tf_op jit(solution)/shard_map/ppermute | solution.py:330
  21.3 2.2 %collective-permute-done.3 = f32[1,8,512]{2,1,0:T(8,128)S(1)} collective-permute-done((f32[1,8,512]{2,1,0:T(8,128)S(1)}, f32[1,8,512]{2,1,0:T(8,128)S(1)}, u32[]{:S(2)}, u32[]{:S(2)}) %collective-permute-start.3) | collective-permute-done | bytes 16416 | tf_op jit(solution)/shard_map/ppermute | solution.py:330
  23.5 0.0 collective-permute-start.4
  23.5 0.9 multiply_select_fusion
  24.4 0.3 collective-permute-done.4
  24.7 0.6 pad_maximum_fusion.2.refs_1_
  25.3 2.8 %codes.1 = bf16[128,256]{1,0:T(8,128)(2,1)} custom-call(s32[1]{0:T(128)} %bitcast.refs_0_, f32[4,8,512]{2,1,0:T(8,128)} %pad_maximum_fusion.2.refs_1_, bf16[80,2048]{1,0:T(8,128)(2,1)} %refs_2_.7, bf16[32,2048]{1,0:T(8,128)(2,1)} %constant_dynamic-slice_fusion.refs_3_, bf16[2048,384]{1,0:T(8,128)(2,1)} %maximum_maximum_fusion.refs_4_, f32[1,256]{1,0:T(1,128)} %bitcast.18, ...), custom_call_target="tpu_custom_call" | custom-call | tf_op jit(solution)/shard_map/codes/pallas_call | solution.py:276
  28.1 0.1 collective-permute-start.8
  28.2 6.7 %collective-permute-done.8 = bf16[1,128,256]{2,1,0:T(8,128)(2,1)S(1)} collective-permute-done((bf16[1,128,256]{2,1,0:T(8,128)(2,1)}, bf16[1,128,256]{2,1,0:T(8,128)(2,1)S(1)}, u32[]{:S(2)}, u32[]{:S(2)}) %collective-permute-start.8) | collective-permute-done | bytes 65568 | tf_op jit(solution)/shard_map/ppermute | solution.py:330
  34.9 0.9 pad_maximum_fusion.1
  35.8 0.3 collective-permute-start.9
  36.1 0.0 collective-permute-start.6
  36.1 1.6 %collective-permute-start.5 = (bf16[80,2048]{1,0:T(8,128)(2,1)S(1)}, bf16[80,2048]{1,0:T(8,128)(2,1)}, u32[]{:S(2)}, u32[]{:S(2)}) collective-permute-start(bf16[80,2048]{1,0:T(8,128)(2,1)S(1)} %copy-done.1), channel_id=1, source_target_pairs={{0,2},{1,3},{2,0},{3,1},{4,6},{5,7},{6,4},{7,5},{8,10},{9,11},{10,... | collective-permute-start | bytes 983048 | tf_op jit(solution)/shard_map/ppermute | solution.py:330
  37.7 3.2 %collective-permute-done.9 = bf16[2,128,256]{2,1,0:T(8,128)(2,1)} collective-permute-done((bf16[2,128,256]{2,1,0:T(8,128)(2,1)S(1)}, bf16[2,128,256]{2,1,0:T(8,128)(2,1)}, u32[]{:S(2)}, u32[]{:S(2)}) %collective-permute-start.9) | collective-permute-done | bytes 131104 | tf_op jit(solution)/shard_map/ppermute | solution.py:330
  40.9 1.0 pad_maximum_fusion.refs_1_
  41.9 1.6 %collective-permute-start.12 = (bf16[4,128,256]{2,1,0:T(8,128)(2,1)S(1)}, bf16[4,128,256]{2,1,0:T(8,128)(2,1)}, u32[]{:S(2)}, u32[]{:S(2)}) collective-permute-start(bf16[4,128,256]{2,1,0:T(8,128)(2,1)S(1)} %pad_maximum_fusion.refs_1_), channel_id=1, source_target_pairs={{0,4},{1,5},{2,6},{3,7},{4,0},{5,1},{6,2},{7,3},{8,12},{9,13},{10,... | collective-permute-start | bytes 786440 | tf_op jit(solution)/shard_map/ppermute | solution.py:330
  43.5 1.5 %collective-permute-start.10 = (bf16[4,128,256]{2,1,0:T(8,128)(2,1)S(1)}, bf16[4,128,256]{2,1,0:T(8,128)(2,1)}, u32[]{:S(2)}, u32[]{:S(2)}) collective-permute-start(bf16[4,128,256]{2,1,0:T(8,128)(2,1)S(1)} %pad_maximum_fusion.refs_1_), channel_id=1, source_target_pairs={{0,2},{1,3},{2,0},{3,1},{4,6},{5,7},{6,4},{7,5},{8,10},{9,11},{10,... | collective-permute-start | bytes 786440 | tf_op jit(solution)/shard_map/ppermute | solution.py:330
  45.0 0.5 iota_add_fusion.3
  45.5 1.4 %collective-permute-done.5.refs_3_ = bf16[80,2048]{1,0:T(8,128)(2,1)} collective-permute-done((bf16[80,2048]{1,0:T(8,128)(2,1)S(1)}, bf16[80,2048]{1,0:T(8,128)(2,1)}, u32[]{:S(2)}, u32[]{:S(2)}) %collective-permute-start.5) | collective-permute-done | bytes 327712 | tf_op jit(solution)/shard_map/ppermute | solution.py:330
  46.9 0.7 add_select_fusion.1
  47.6 0.0 collective-permute-done.6.refs_4_
  47.6 0.0 copy-start.3
  47.6 0.6 collective-permute-start.18
  48.2 0.2 collective-permute-done.12.refs_1_
  48.5 3.5 %collective-permute-done.10.refs_2_ = bf16[4,128,256]{2,1,0:T(8,128)(2,1)} collective-permute-done((bf16[4,128,256]{2,1,0:T(8,128)(2,1)S(1)}, bf16[4,128,256]{2,1,0:T(8,128)(2,1)}, u32[]{:S(2)}, u32[]{:S(2)}) %collective-permute-start.10) | collective-permute-done | bytes 262176 | tf_op jit(solution)/shard_map/ppermute | solution.py:330
  52.0 0.0 collective-permute-start.17
  52.0 1.9 %sine_multiply_fusion = (f32[320,128]{1,0:T(8,128)}, f32[320,128]{1,0:T(8,128)}) fusion(f32[128]{0:T(128)S(1)} %get-tuple-element.21, f32[128]{0:T(128)S(1)} %get-tuple-element.22, s32[320]{0:T(512)S(1)} %get-tuple-element.18, s32[320]{0:T(512)S(1)} %get-tuple-element.17, pred[128]{0:T(512)(128)(4,1)S(1)} %fusion.3), kind=kLoop, calls=%fused_computation.2 | loop fusion | flops 163840 | bytes 331392 | tf_op jit(solution)/shard_map/mul | solution.py:296
  53.9 0.9 slice.9
  54.8 0.9 slice.8
  55.7 0.0 collective-permute-done.7.refs_5_
  55.7 1.6 %collective-permute-start.13 = (bf16[2,128,256]{2,1,0:T(8,128)(2,1)S(1)}, bf16[2,128,256]{2,1,0:T(8,128)(2,1)S(1)}, u32[]{:S(2)}, u32[]{:S(2)}) collective-permute-start(bf16[2,128,256]{2,1,0:T(8,128)(2,1)S(1)} %slice.9), channel_id=1, source_target_pairs={{0,2},{1,3},{2,0},{3,1},{4,6},{5,7},{6,4},{7,5},{8,10},{9,11},{10,... | collective-permute-start | bytes 393224 | tf_op jit(solution)/shard_map/ppermute | solution.py:330
  57.3 3.6 %gate.1.refs_8_ = bf16[320,512]{1,0:T(8,128)(2,1)} custom-call(s32[1]{0:T(128)} %bitcast.refs_0_, f32[4,8,512]{2,1,0:T(8,128)} %pad_maximum_fusion.2.refs_1_, bf16[80,2048]{1,0:T(8,128)(2,1)} %refs_2_.7, bf16[80,2048]{1,0:T(8,128)(2,1)} %collective-permute-done.5.refs_3_, bf16[80,2048]{1,0:T(8,128)(2,1)} %copy-done.3, bf16[80,2048]{1,0:T(8,128)(2,1)} %copy-done.4, ...), custom_call_target="tpu_custom_call" | custom-call | flops 671088640 | tf_op jit(solution)/shard_map/gate/pallas_call | solution.py:276
  60.9 1.6 %collective-permute-start.11 = (bf16[2,128,256]{2,1,0:T(8,128)(2,1)S(1)}, bf16[2,128,256]{2,1,0:T(8,128)(2,1)S(1)}, u32[]{:S(2)}, u32[]{:S(2)}) collective-permute-start(bf16[2,128,256]{2,1,0:T(8,128)(2,1)S(1)} %slice.8), channel_id=1, source_target_pairs={{0,4},{1,5},{2,6},{3,7},{4,0},{5,1},{6,2},{7,3},{8,12},{9,13},{10,... | collective-permute-start | bytes 393224 | tf_op jit(solution)/shard_map/ppermute | solution.py:330
  62.5 4.8 %queries.1.refs_0_ = bf16[8,320,128]{2,1,0:T(8,128)(2,1)} custom-call(s32[1]{0:T(128)} %bitcast.refs_0_, f32[4,8,512]{2,1,0:T(8,128)} %pad_maximum_fusion.2.refs_1_, bf16[80,2048]{1,0:T(8,128)(2,1)} %refs_2_.7, bf16[80,2048]{1,0:T(8,128)(2,1)} %collective-permute-done.5.refs_3_, bf16[80,2048]{1,0:T(8,128)(2,1)} %copy-done.3, bf16[80,2048]{1,0:T(8,128)(2,1)} %copy-done.4, ...), custom_call_target="tpu_custom_call" | custom-call | flops 671088640 | tf_op jit(solution)/shard_map/queries/pallas_call | solution.py:276
  67.3 8.6 %attend.3.refs_7_ = f32[8,320,128]{2,1,0:T(8,128)} custom-call(bf16[8,320,128]{2,1,0:T(8,128)(2,1)} %queries.1.refs_0_, bf16[4,128,256]{2,1,0:T(8,128)(2,1)} %copy-done.6, bf16[4,128,256]{2,1,0:T(8,128)(2,1)} %copy-done.12, bf16[256,512]{1,0:T(8,128)(2,1)} %refs_5_.3, bf16[256,512]{1,0:T(8,128)(2,1)} %refs_6_.7), custom_call_target="tpu_custom_call" | custom-call | flops 1174405120 | bytes 1048576 | tf_op jit(solution)/shard_map/attend/pallas_call | solution.py:245
  75.9 0.1 collective-permute-start.15
  76.0 0.5 collective-permute-start.14
  76.5 0.7 copy-done.10
  77.2 0.7 copy-done.11
  77.9 13.1 %attend.4.refs_7_ = f32[8,320,128]{2,1,0:T(8,128)} custom-call(bf16[8,320,128]{2,1,0:T(8,128)(2,1)} %queries.1.refs_0_, bf16[4,128,256]{2,1,0:T(8,128)(2,1)} %collective-permute-done.12.refs_1_, bf16[4,128,256]{2,1,0:T(8,128)(2,1)} %collective-permute-done.10.refs_2_, bf16[4,128,256]{2,1,0:T(8,128)(2,1)} %copy-done.10, bf16[4,128,256]{2,1,0:T(8,128)(2,1)} %copy-done.11, ...), custom_call_target="tpu_custom_call" | custom-call | flops 2348810240 | bytes 1048576 | tf_op jit(solution)/shard_map/attend/pallas_call | solution.py:245
  91.0 0.6 copy-done.15
  91.6 0.7 copy-done.16
  92.3 10.1 %attend.5 = (bf16[160,512]{1,0:T(8,128)(2,1)}, bf16[160,512]{1,0:T(8,128)(2,1)}) custom-call(bf16[8,320,128]{2,1,0:T(8,128)(2,1)} %queries.1.refs_0_, bf16[2,128,256]{2,1,0:T(8,128)(2,1)} %copy-done.14, bf16[2,128,256]{2,1,0:T(8,128)(2,1)} %copy-done.13, bf16[2,128,256]{2,1,0:T(8,128)(2,1)} %copy-done.16, bf16[2,128,256]{2,1,0:T(8,128)(2,1)} %copy-done.15, ...), custom_call_target="tpu_custom_call" | custom-call | flops 1174405120 | bytes 1048576 | tf_op jit(solution)/shard_map/attend/pallas_call | solution.py:245
  102.4 0.1 collective-permute-start.19
  102.5 1.5 %collective-permute-done.19.theirs_ref = bf16[160,512]{1,0:T(8,128)(2,1)S(1)} collective-permute-done((bf16[160,512]{1,0:T(8,128)(2,1)}, bf16[160,512]{1,0:T(8,128)(2,1)S(1)}, u32[]{:S(2)}, u32[]{:S(2)}) %collective-permute-start.19) | collective-permute-done | bytes 163872 | tf_op jit(solution)/shard_map/ppermute | solution.py:330
  104.1 0.7 copy-done.8
  104.7 0.7 copy-done.2
  105.4 4.8 %branch.1 = (bf16[80,2048]{1,0:T(8,128)(2,1)}, f32[80,2048]{1,0:T(8,128)}) custom-call(bf16[160,512]{1,0:T(8,128)(2,1)} %get-tuple-element.9.mine_ref, bf16[160,512]{1,0:T(8,128)(2,1)} %copy-done.8, bf16[512,2048]{1,0:T(8,128)(2,1)} %w_mine_ref.1, bf16[512,2048]{1,0:T(8,128)(2,1)} %copy-done.2), custom_call_target="tpu_custom_call" | custom-call | flops 671088640 | tf_op jit(solution)/shard_map/branch/pallas_call | solution.py:276
  110.3 0.6 collective-permute-start.21
  110.9 9.3 %collective-permute-done.21.refs_4_ = bf16[80,2048]{1,0:T(8,128)(2,1)S(1)} collective-permute-done((bf16[80,2048]{1,0:T(8,128)(2,1)}, bf16[80,2048]{1,0:T(8,128)(2,1)S(1)}, u32[]{:S(2)}, u32[]{:S(2)}) %collective-permute-start.21) | collective-permute-done | bytes 327712 | tf_op jit(solution)/shard_map/ppermute | solution.py:330
  120.3 0.7 copy-done.5
  121.0 2.4 %norm.1 = bf16[80,2048]{1,0:T(8,128)(2,1)} custom-call(s32[1]{0:T(128)} %bitcast.refs_0_, f32[4,8,512]{2,1,0:T(8,128)} %pad_maximum_fusion.2.refs_1_, bf16[80,2048]{1,0:T(8,128)(2,1)} %refs_2_.7, f32[80,2048]{1,0:T(8,128)} %get-tuple-element.11.refs_3_, bf16[80,2048]{1,0:T(8,128)(2,1)} %copy-done.5, f32[1,2048]{1,0:T(1,128)} %bitcast.13, f32[1,2048]{1,0:T(1,128)} %bitcast.14), custom_call_target="tpu_custom_call" | custom-call | tf_op jit(solution)/shard_map/norm/pallas_call | solution.py:276
  (49 shorter events, 0.1 us)
Async XLA Ops:
  0.0 8.7 %copy-start = (bf16[128,2048]{1,0:T(8,128)(2,1)S(1)}, bf16[128,2048]{1,0:T(8,128)(2,1)}, u32[]{:S(2)}) copy-start(bf16[128,2048]{1,0:T(8,128)(2,1)} %param.21) | copy-start | bytes 1572868
  3.4 8.8 %copy-start.9 = (f32[8,512]{1,0:T(8,128)S(1)}, f32[8,512]{1,0:T(8,128)}, u32[]{:S(2)}) copy-start(f32[8,512]{1,0:T(8,128)} %mod.1) | copy-start | bytes 49156
  3.4 8.8 %collective-permute-start = (f32[8,512]{1,0:T(8,128)}, f32[8,512]{1,0:T(8,128)S(1)}, u32[]{:S(2)}, u32[]{:S(2)}) collective-permute-start(f32[8,512]{1,0:T(8,128)} %mod.1), channel_id=1, source_target_pairs={{0,16},{1,17},{2,18},{3,19},{4,20},{5,21},{6,22},{7,23},{8,24},{9,... | collective-permute-start | bytes 49160 | tf_op jit(solution)/shard_map/ppermute | solution.py:330
  7.4 96.6 %collective-permute-start.20 = (bf16[512,2048]{1,0:T(8,128)(2,1)}, bf16[512,2048]{1,0:T(8,128)(2,1)S(1)}, u32[]{:S(2)}, u32[]{:S(2)}) collective-permute-start(bf16[512,2048]{1,0:T(8,128)(2,1)} %w_mine_ref.1), channel_id=1, source_target_pairs={{0,1},{1,0},{2,3},{3,2},{4,5},{5,4},{6,7},{7,6},{8,9},{9,8},{10,11... | collective-permute-start | bytes 6291464 | tf_op jit(solution)/shard_map/ppermute | solution.py:330
  12.1 24.0 %copy-start.1 = (bf16[80,2048]{1,0:T(8,128)(2,1)S(1)}, bf16[80,2048]{1,0:T(8,128)(2,1)}, u32[]{:S(2)}) copy-start(bf16[80,2048]{1,0:T(8,128)(2,1)} %refs_2_.7) | copy-start | bytes 983044
  12.2 3.8 %collective-permute-start.1 = (f32[8,512]{1,0:T(8,128)S(1)}, f32[8,512]{1,0:T(8,128)S(1)}, u32[]{:S(2)}, u32[]{:S(2)}) collective-permute-start(f32[8,512]{1,0:T(8,128)S(1)} %add.157), channel_id=1, source_target_pairs={{0,8},{1,9},{2,10},{3,11},{4,12},{5,13},{6,14},{7,15},{8,0},{9,1},... | collective-permute-start | bytes 49160 | tf_op jit(solution)/shard_map/ppermute | solution.py:330
  16.0 3.7 %collective-permute-start.2 = (f32[8,512]{1,0:T(8,128)S(1)}, f32[8,512]{1,0:T(8,128)S(1)}, u32[]{:S(2)}, u32[]{:S(2)}) collective-permute-start(f32[8,512]{1,0:T(8,128)S(1)} %add.158), channel_id=1, source_target_pairs={{0,4},{1,5},{2,6},{3,7},{4,0},{5,1},{6,2},{7,3},{8,12},{9,13},{10,... | collective-permute-start | bytes 49160 | tf_op jit(solution)/shard_map/ppermute | solution.py:330
  19.8 3.7 %collective-permute-start.3 = (f32[1,8,512]{2,1,0:T(8,128)S(1)}, f32[1,8,512]{2,1,0:T(8,128)S(1)}, u32[]{:S(2)}, u32[]{:S(2)}) collective-permute-start(f32[1,8,512]{2,1,0:T(8,128)S(1)} %add_bitcast_fusion), channel_id=1, source_target_pairs={{0,2},{1,3},{2,0},{3,1},{4,6},{5,7},{6,4},{7,5},{8,10},{9,11},{10,... | collective-permute-start | bytes 49160 | tf_op jit(solution)/shard_map/ppermute | solution.py:330
  23.5 1.2 collective-permute-start.4
  28.1 6.8 %collective-permute-start.8 = (bf16[1,128,256]{2,1,0:T(8,128)(2,1)}, bf16[1,128,256]{2,1,0:T(8,128)(2,1)S(1)}, u32[]{:S(2)}, u32[]{:S(2)}) collective-permute-start(bf16[1,128,256]{2,1,0:T(8,128)(2,1)} %bitcast.10), channel_id=1, source_target_pairs={{0,16},{1,17},{2,18},{3,19},{4,20},{5,21},{6,22},{7,23},{8,24},{9,... | collective-permute-start | bytes 196616 | tf_op jit(solution)/shard_map/ppermute | solution.py:330
  34.9 1.2 copy-start.7
  35.8 5.1 %collective-permute-start.9 = (bf16[2,128,256]{2,1,0:T(8,128)(2,1)S(1)}, bf16[2,128,256]{2,1,0:T(8,128)(2,1)}, u32[]{:S(2)}, u32[]{:S(2)}) collective-permute-start(bf16[2,128,256]{2,1,0:T(8,128)(2,1)S(1)} %pad_maximum_fusion.1), channel_id=1, source_target_pairs={{0,8},{1,9},{2,10},{3,11},{4,12},{5,13},{6,14},{7,15},{8,0},{9,1},... | collective-permute-start | bytes 393224 | tf_op jit(solution)/shard_map/ppermute | solution.py:330
  36.1 11.5 %collective-permute-start.6 = (bf16[80,2048]{1,0:T(8,128)(2,1)S(1)}, bf16[80,2048]{1,0:T(8,128)(2,1)S(1)}, u32[]{:S(2)}, u32[]{:S(2)}) collective-permute-start(bf16[80,2048]{1,0:T(8,128)(2,1)S(1)} %copy-done.1), channel_id=1, source_target_pairs={{0,1},{1,0},{2,3},{3,2},{4,5},{5,4},{6,7},{7,6},{8,9},{9,8},{10,11... | collective-permute-start | bytes 983048 | tf_op jit(solution)/shard_map/ppermute | solution.py:330
  36.1 10.8 %collective-permute-start.5 = (bf16[80,2048]{1,0:T(8,128)(2,1)S(1)}, bf16[80,2048]{1,0:T(8,128)(2,1)}, u32[]{:S(2)}, u32[]{:S(2)}) collective-permute-start(bf16[80,2048]{1,0:T(8,128)(2,1)S(1)} %copy-done.1), channel_id=1, source_target_pairs={{0,2},{1,3},{2,0},{3,1},{4,6},{5,7},{6,4},{7,5},{8,10},{9,11},{10,... | collective-permute-start | bytes 983048 | tf_op jit(solution)/shard_map/ppermute | solution.py:330
  41.9 19.0 %copy-start.6 = (bf16[4,128,256]{2,1,0:T(8,128)(2,1)}, bf16[4,128,256]{2,1,0:T(8,128)(2,1)S(1)}, u32[]{:S(2)}) copy-start(bf16[4,128,256]{2,1,0:T(8,128)(2,1)S(1)} %pad_maximum_fusion.refs_1_) | copy-start | bytes 786436
  41.9 6.5 %collective-permute-start.12 = (bf16[4,128,256]{2,1,0:T(8,128)(2,1)S(1)}, bf16[4,128,256]{2,1,0:T(8,128)(2,1)}, u32[]{:S(2)}, u32[]{:S(2)}) collective-permute-start(bf16[4,128,256]{2,1,0:T(8,128)(2,1)S(1)} %pad_maximum_fusion.refs_1_), channel_id=1, source_target_pairs={{0,4},{1,5},{2,6},{3,7},{4,0},{5,1},{6,2},{7,3},{8,12},{9,13},{10,... | collective-permute-start | bytes 786440 | tf_op jit(solution)/shard_map/ppermute | solution.py:330
  43.5 8.5 %collective-permute-start.10 = (bf16[4,128,256]{2,1,0:T(8,128)(2,1)S(1)}, bf16[4,128,256]{2,1,0:T(8,128)(2,1)}, u32[]{:S(2)}, u32[]{:S(2)}) collective-permute-start(bf16[4,128,256]{2,1,0:T(8,128)(2,1)S(1)} %pad_maximum_fusion.refs_1_), channel_id=1, source_target_pairs={{0,2},{1,3},{2,0},{3,1},{4,6},{5,7},{6,4},{7,5},{8,10},{9,11},{10,... | collective-permute-start | bytes 786440 | tf_op jit(solution)/shard_map/ppermute | solution.py:330
  46.9 8.8 %collective-permute-start.7 = (bf16[80,2048]{1,0:T(8,128)(2,1)}, bf16[80,2048]{1,0:T(8,128)(2,1)S(1)}, u32[]{:S(2)}, u32[]{:S(2)}) collective-permute-start(bf16[80,2048]{1,0:T(8,128)(2,1)} %collective-permute-done.5.refs_3_), channel_id=1, source_target_pairs={{0,1},{1,0},{2,3},{3,2},{4,5},{5,4},{6,7},{7,6},{8,9},{9,8},{10,11... | collective-permute-start | bytes 983048 | tf_op jit(solution)/shard_map/ppermute | solution.py:330
  47.6 9.7 %copy-start.3 = (bf16[80,2048]{1,0:T(8,128)(2,1)}, bf16[80,2048]{1,0:T(8,128)(2,1)S(1)}, u32[]{:S(2)}) copy-start(bf16[80,2048]{1,0:T(8,128)(2,1)S(1)} %collective-permute-done.6.refs_4_) | copy-start | bytes 983044
  47.6 13.3 %collective-permute-start.18 = (bf16[4,128,256]{2,1,0:T(8,128)(2,1)S(1)}, bf16[4,128,256]{2,1,0:T(8,128)(2,1)S(1)}, u32[]{:S(2)}, u32[]{:S(2)}) collective-permute-start(bf16[4,128,256]{2,1,0:T(8,128)(2,1)S(1)} %pad_maximum_fusion.refs_1_), channel_id=1, source_target_pairs={{0,1},{1,0},{2,3},{3,2},{4,5},{5,4},{6,7},{7,6},{8,9},{9,8},{10,11... | collective-permute-start | bytes 786440 | tf_op jit(solution)/shard_map/ppermute | solution.py:330
  48.5 28.0 %collective-permute-start.16 = (bf16[4,128,256]{2,1,0:T(8,128)(2,1)}, bf16[4,128,256]{2,1,0:T(8,128)(2,1)S(1)}, u32[]{:S(2)}, u32[]{:S(2)}) collective-permute-start(bf16[4,128,256]{2,1,0:T(8,128)(2,1)} %collective-permute-done.12.refs_1_), channel_id=1, source_target_pairs={{0,1},{1,0},{2,3},{3,2},{4,5},{5,4},{6,7},{7,6},{8,9},{9,8},{10,11... | collective-permute-start | bytes 786440 | tf_op jit(solution)/shard_map/ppermute | solution.py:330
  52.0 24.5 %collective-permute-start.17 = (bf16[4,128,256]{2,1,0:T(8,128)(2,1)}, bf16[4,128,256]{2,1,0:T(8,128)(2,1)S(1)}, u32[]{:S(2)}, u32[]{:S(2)}) collective-permute-start(bf16[4,128,256]{2,1,0:T(8,128)(2,1)} %collective-permute-done.10.refs_2_), channel_id=1, source_target_pairs={{0,1},{1,0},{2,3},{3,2},{4,5},{5,4},{6,7},{7,6},{8,9},{9,8},{10,11... | collective-permute-start | bytes 786440 | tf_op jit(solution)/shard_map/ppermute | solution.py:330
  55.7 1.6 %copy-start.4 = (bf16[80,2048]{1,0:T(8,128)(2,1)}, bf16[80,2048]{1,0:T(8,128)(2,1)S(1)}, u32[]{:S(2)}) copy-start(bf16[80,2048]{1,0:T(8,128)(2,1)S(1)} %collective-permute-done.7.refs_5_) | copy-start | bytes 983044
  55.7 20.1 %collective-permute-start.13 = (bf16[2,128,256]{2,1,0:T(8,128)(2,1)S(1)}, bf16[2,128,256]{2,1,0:T(8,128)(2,1)S(1)}, u32[]{:S(2)}, u32[]{:S(2)}) collective-permute-start(bf16[2,128,256]{2,1,0:T(8,128)(2,1)S(1)} %slice.9), channel_id=1, source_target_pairs={{0,2},{1,3},{2,0},{3,1},{4,6},{5,7},{6,4},{7,5},{8,10},{9,11},{10,... | collective-permute-start | bytes 393224 | tf_op jit(solution)/shard_map/ppermute | solution.py:330
  60.9 6.4 %copy-start.12 = (bf16[4,128,256]{2,1,0:T(8,128)(2,1)}, bf16[4,128,256]{2,1,0:T(8,128)(2,1)S(1)}, u32[]{:S(2)}) copy-start(bf16[4,128,256]{2,1,0:T(8,128)(2,1)S(1)} %collective-permute-done.18.refs_2_) | copy-start | bytes 786436
  60.9 15.1 %collective-permute-start.11 = (bf16[2,128,256]{2,1,0:T(8,128)(2,1)S(1)}, bf16[2,128,256]{2,1,0:T(8,128)(2,1)S(1)}, u32[]{:S(2)}, u32[]{:S(2)}) collective-permute-start(bf16[2,128,256]{2,1,0:T(8,128)(2,1)S(1)} %slice.8), channel_id=1, source_target_pairs={{0,4},{1,5},{2,6},{3,7},{4,0},{5,1},{6,2},{7,3},{8,12},{9,13},{10,... | collective-permute-start | bytes 393224 | tf_op jit(solution)/shard_map/ppermute | solution.py:330
  75.9 15.1 %copy-start.13 = (bf16[2,128,256]{2,1,0:T(8,128)(2,1)}, bf16[2,128,256]{2,1,0:T(8,128)(2,1)S(1)}, u32[]{:S(2)}) copy-start(bf16[2,128,256]{2,1,0:T(8,128)(2,1)S(1)} %collective-permute-done.13.refs_2_) | copy-start | bytes 393220
  75.9 15.1 %collective-permute-start.15 = (bf16[2,128,256]{2,1,0:T(8,128)(2,1)S(1)}, bf16[2,128,256]{2,1,0:T(8,128)(2,1)S(1)}, u32[]{:S(2)}, u32[]{:S(2)}) collective-permute-start(bf16[2,128,256]{2,1,0:T(8,128)(2,1)S(1)} %collective-permute-done.13.refs_2_), channel_id=1, source_target_pairs={{0,1},{1,0},{2,3},{3,2},{4,5},{5,4},{6,7},{7,6},{8,9},{9,8},{10,11... | collective-permute-start | bytes 393224 | tf_op jit(solution)/shard_map/ppermute | solution.py:330
  76.0 15.0 %copy-start.14 = (bf16[2,128,256]{2,1,0:T(8,128)(2,1)}, bf16[2,128,256]{2,1,0:T(8,128)(2,1)S(1)}, u32[]{:S(2)}) copy-start(bf16[2,128,256]{2,1,0:T(8,128)(2,1)S(1)} %collective-permute-done.11.refs_1_) | copy-start | bytes 393220
  76.0 15.0 %collective-permute-start.14 = (bf16[2,128,256]{2,1,0:T(8,128)(2,1)S(1)}, bf16[2,128,256]{2,1,0:T(8,128)(2,1)S(1)}, u32[]{:S(2)}, u32[]{:S(2)}) collective-permute-start(bf16[2,128,256]{2,1,0:T(8,128)(2,1)S(1)} %collective-permute-done.11.refs_1_), channel_id=1, source_target_pairs={{0,1},{1,0},{2,3},{3,2},{4,5},{5,4},{6,7},{7,6},{8,9},{9,8},{10,11... | collective-permute-start | bytes 393224 | tf_op jit(solution)/shard_map/ppermute | solution.py:330
  76.5 0.7 copy-start.10
  77.2 0.7 copy-start.11
  91.0 0.7 copy-start.15
  91.6 0.7 copy-start.16
  102.4 1.6 %collective-permute-start.19 = (bf16[160,512]{1,0:T(8,128)(2,1)}, bf16[160,512]{1,0:T(8,128)(2,1)S(1)}, u32[]{:S(2)}, u32[]{:S(2)}) collective-permute-start(bf16[160,512]{1,0:T(8,128)(2,1)} %get-tuple-element.10), channel_id=1, source_target_pairs={{0,1},{1,0},{2,3},{3,2},{4,5},{5,4},{6,7},{7,6},{8,9},{9,8},{10,11... | collective-permute-start | bytes 491528 | tf_op jit(solution)/shard_map/ppermute | solution.py:330
  104.1 0.7 copy-start.8
  104.1 1.4 %copy-start.2 = (bf16[512,2048]{1,0:T(8,128)(2,1)}, bf16[512,2048]{1,0:T(8,128)(2,1)S(1)}, u32[]{:S(2)}) copy-start(bf16[512,2048]{1,0:T(8,128)(2,1)S(1)} %collective-permute-done.20.w_theirs_ref) | copy-start | bytes 6291460
  110.3 10.0 %collective-permute-start.21 = (bf16[80,2048]{1,0:T(8,128)(2,1)}, bf16[80,2048]{1,0:T(8,128)(2,1)S(1)}, u32[]{:S(2)}, u32[]{:S(2)}) collective-permute-start(bf16[80,2048]{1,0:T(8,128)(2,1)} %get-tuple-element.12), channel_id=1, source_target_pairs={{0,2},{1,3},{2,0},{3,1},{4,6},{5,7},{6,4},{7,5},{8,10},{9,11},{10,... | collective-permute-start | bytes 983048 | tf_op jit(solution)/shard_map/ppermute | solution.py:330
  120.3 0.7 copy-start.5
